TPU v7x, 32 devices: a whole 2x2x4 slice. The times are simulated.
32 devices in a mesh: sp: 8 (over z, x), tp: 4 (over y, core).
Axes of the slice: x: 2, y: 2, z: 4, core: 2. Of those that a mesh axis runs over, the one named last changes fastest.
Arguments:
- residual: bfloat16 [2048, 2048], P(('sp', 'tp')), may hold values from -6 to 6
- query_wide: bfloat16 [2048, 512], P('sp', 'tp'), may hold values from -8 to 8
- key_wide: bfloat16 [2048, 512], P('sp', 'tp'), may hold values from -8 to 8
- value_wide: bfloat16 [2048, 512], P('sp', 'tp'), may hold values from -6 to 6
- query_narrow: bfloat16 [2048, 512], P('sp', 'tp'), may hold values from -8 to 8
- key_narrow: bfloat16 [2048, 512], P('sp', 'tp'), may hold values from -8 to 8
- value_narrow: bfloat16 [2048, 512], P('sp', 'tp'), may hold values from -6 to 6
- gate_wide: float32 [2048, 4], P('sp', 'tp'), may hold values from -2 to 20
- gate_narrow: float32 [2048, 8], P('sp', 'tp'), may hold values from -2 to 20
- out_wide: bfloat16 [512, 2048], replicated, may hold values from -0.1875 to 0.1875
- out_narrow: bfloat16 [512, 2048], replicated, may hold values from -0.1875 to 0.1875
- norm_gain: float32 [2048], replicated, may hold values from 0.1 to 1.9
- routing: int32 [2048, 2], P(('sp', 'tp')), may hold values from 0 to 7, as said below
- route_weight: float32 [2048, 2], P(('sp', 'tp')), may hold values from 0.3 to 1.5
- gate_weight: bfloat16 [8, 2048, 1024], P('sp', None, 'tp'), may hold values from -0.125 to 0.125
- up_weight: bfloat16 [8, 2048, 1024], P('sp', None, 'tp'), may hold values from -0.125 to 0.125
- down_weight: bfloat16 [8, 1024, 2048], P('sp', 'tp'), may hold values from -0.1875 to 0.1875
Outputs:
- result: bfloat16 [2048, 2048], P(('sp', 'tp'))
Inputs may be any that keep to these rules, and one draw needn't show every extreme that they name: `routing`: each row names 2 different experts of one group (experts g * 2 to g * 2 + 1). In each aligned block of 64 rows (the rows of one device) no expert is named by more than 32 rows; one group, the same for all blocks, has each of its experts named by exactly 32 rows of every block.
All inputs are finite; a program needn't handle non-finite values.
Results may differ from a plain program's by a relative error of at most 0.017.
Values may be sent and summed in bfloat16 or wider, within the bound.
A program may use at most 128 MiB of HBM per device.

v0:
```python
import math
import jax
import jax.numpy as jnp
from jax import lax
from jax.sharding import PartitionSpec as P

HW = 128
HN = 64
GROUPS = 4
epsilon = 1e-06


def globalize(pieces, shard_rows):
    shards = pieces.shape[0] // shard_rows
    grid = pieces.reshape(shards, shard_rows, pieces.shape[1])
    endings = grid[:, -1, :]
    offsets = jnp.cumsum(endings, axis=0) - endings
    return (grid + offsets[:, None, :]).reshape(pieces.shape)


def head_block(
    state, queries, query_decay, keys, values, key_decay, first_key, first_query, head_width
):
    highest_old, weight_sum, weighted = state
    query_rows = queries.shape[0]
    head_count = query_decay.shape[1]
    key_rows = keys.shape[0]
    grid_query = queries.reshape(query_rows, head_count, head_width)
    grid_key = keys.reshape(key_rows, head_count, head_width)
    grid_value = values.reshape(key_rows, head_count, head_width)
    scores = jnp.einsum("thd,phd->htp", grid_query, grid_key, preferred_element_type=jnp.float32)
    scores = scores * head_width ** (-0.5) + query_decay.T[:, :, None] - key_decay.T[:, None, :]
    query_place = first_query + jnp.arange(query_rows, dtype=jnp.int32)
    key_place = first_key + jnp.arange(key_rows, dtype=jnp.int32)
    scores = jnp.where(key_place[None, None, :] <= query_place[None, :, None], scores, -jnp.inf)
    highest = jnp.maximum(highest_old, jnp.max(scores, axis=2))
    weights = jnp.exp(scores - highest[:, :, None])
    shrink = jnp.exp(highest_old - highest)
    weight_sum = weight_sum * shrink + jnp.sum(weights, axis=2)
    product = jnp.einsum(
        "htp,phd->htd", weights.astype(jnp.bfloat16), grid_value, preferred_element_type=jnp.float32
    )
    weighted = weighted * shrink[:, :, None] + product
    return (highest, weight_sum, weighted)


def fresh_state(head_count, shard_rows, head_width):
    return (
        jnp.full((head_count, shard_rows), -1e30, jnp.float32),
        jnp.zeros((head_count, shard_rows), jnp.float32),
        jnp.zeros((head_count, shard_rows, head_width), jnp.float32),
    )


def finish(state, shard_rows):
    highest, weight_sum, weighted = state
    mixed_heads = weighted / weight_sum[:, :, None]
    joined = jnp.transpose(mixed_heads, (1, 0, 2))
    return joined.reshape(shard_rows, weighted.shape[0] * weighted.shape[2]).astype(jnp.bfloat16)


def body(
    residual,
    query_wide,
    key_wide,
    value_wide,
    query_narrow,
    key_narrow,
    value_narrow,
    gate_wide,
    gate_narrow,
    out_wide,
    out_narrow,
    norm_gain,
    routing,
    route_weight,
    gate_weight,
    up_weight,
    down_weight,
):
    shard_rows = query_wide.shape[0]
    half_rows = shard_rows // 2
    sp_place = lax.axis_index("sp")
    first_query = sp_place * shard_rows
    running_wide = jnp.cumsum(jax.nn.log_sigmoid(gate_wide), axis=0)
    running_narrow = jnp.cumsum(jax.nn.log_sigmoid(gate_narrow), axis=0)
    pieces_wide, pieces_narrow = (
        lax.all_gather(running_wide, "sp", axis=0, tiled=True),
        lax.all_gather(running_narrow, "sp", axis=0, tiled=True),
    )
    every_wide = globalize(pieces_wide, shard_rows)
    every_narrow = globalize(pieces_narrow, shard_rows)
    late_first = first_query + half_rows
    halves = []
    for place, part_wide, part_narrow in (
        (first_query, query_wide[:half_rows], query_narrow[:half_rows]),
        (late_first, query_wide[half_rows:], query_narrow[half_rows:]),
    ):
        halves.append(
            (
                place,
                part_wide,
                part_narrow,
                lax.dynamic_slice_in_dim(every_wide, place, half_rows, 0),
                lax.dynamic_slice_in_dim(every_narrow, place, half_rows, 0),
            )
        )

    def half_state():
        return (
            fresh_state(gate_wide.shape[1], half_rows, HW),
            fresh_state(gate_narrow.shape[1], half_rows, HN),
        )

    state = (half_state(), half_state())
    keys_wide = lax.all_gather(key_wide, "sp", axis=0, tiled=True)
    values_wide = lax.all_gather(value_wide, "sp", axis=0, tiled=True)
    keys_narrow = lax.all_gather(key_narrow, "sp", axis=0, tiled=True)
    values_narrow = lax.all_gather(value_narrow, "sp", axis=0, tiled=True)
    span_rows = keys_wide.shape[0]
    block_size = math.gcd(span_rows, 2048)

    def visit(carried, position):
        inside = position * block_size

        def take_block(source):
            return lax.dynamic_slice_in_dim(source, inside, block_size, 0)

        def take_decay(source):
            return lax.dynamic_slice_in_dim(source, inside, block_size, 0)

        block_kw = take_block(keys_wide)
        block_vw = take_block(values_wide)
        block_kn = take_block(keys_narrow)
        block_vn = take_block(values_narrow)
        block_dw = take_decay(every_wide)
        block_dn = take_decay(every_narrow)

        def one_half(current, half):
            place, part_wide, part_narrow, query_decay_wide, query_decay_narrow = half

            def work(inner):
                first = head_block(
                    inner[0],
                    part_wide,
                    query_decay_wide,
                    block_kw,
                    block_vw,
                    block_dw,
                    inside,
                    place,
                    HW,
                )
                second = head_block(
                    inner[1],
                    part_narrow,
                    query_decay_narrow,
                    block_kn,
                    block_vn,
                    block_dn,
                    inside,
                    place,
                    HN,
                )
                return (first, second)

            def skip(inner):
                return inner

            return lax.cond(inside <= place + half_rows - 1, work, skip, current)

        updated = (one_half(carried[0], halves[0]), one_half(carried[1], halves[1]))
        return (updated, None)

    state, _ = lax.scan(visit, state, jnp.arange(span_rows // block_size, dtype=jnp.int32))
    att_wide = jnp.concatenate(
        [finish(state[0][0], half_rows), finish(state[1][0], half_rows)], axis=0
    )
    att_narrow = jnp.concatenate(
        [finish(state[0][1], half_rows), finish(state[1][1], half_rows)], axis=0
    )
    own_rows = residual.shape[0]
    tp_place = lax.axis_index("tp")
    rows_wide = lax.dynamic_slice_in_dim(
        out_wide, tp_place * att_wide.shape[1], att_wide.shape[1], 0
    )
    rows_narrow = lax.dynamic_slice_in_dim(
        out_narrow, tp_place * att_narrow.shape[1], att_narrow.shape[1], 0
    )
    first = jnp.dot(att_wide, rows_wide, preferred_element_type=jnp.float32)
    second = jnp.dot(att_narrow, rows_narrow, preferred_element_type=jnp.float32)
    mixed = lax.psum_scatter(
        (first + second).astype(jnp.bfloat16), "tp", scatter_dimension=0, tiled=True
    ).astype(jnp.float32)
    middle = (residual.astype(jnp.float32) + mixed).astype(jnp.bfloat16)
    middle_wide = middle.astype(jnp.float32)
    spread = jnp.mean(middle_wide * middle_wide, axis=1, keepdims=True)
    normed = (middle_wide * lax.rsqrt(spread + epsilon) * norm_gain).astype(jnp.bfloat16)
    features = normed.shape[1]
    chosen_count = routing.shape[1]
    expert_count = gate_weight.shape[0] * lax.axis_size("sp")
    capacity = own_rows * GROUPS // expert_count
    flat_routes = routing.reshape(-1)
    matches = (flat_routes[:, None] == jnp.arange(expert_count, dtype=jnp.int32)[None, :]).astype(
        jnp.int32
    )
    ranking = jnp.sum((jnp.cumsum(matches, axis=0) - matches) * matches, axis=1)
    placing = flat_routes * capacity + ranking
    picker = (
        placing[None, :] == jnp.arange(expert_count * capacity, dtype=jnp.int32)[:, None]
    ).astype(jnp.bfloat16)
    picker = jnp.sum(picker.reshape(expert_count * capacity, own_rows, chosen_count), axis=2)
    outgoing = jnp.dot(picker, normed, preferred_element_type=jnp.float32).astype(jnp.bfloat16)
    outgoing = outgoing.reshape(expert_count, capacity, features)
    arrived = lax.all_to_all(outgoing, "sp", split_axis=0, concat_axis=0, tiled=True)
    pooled = lax.all_gather(arrived.reshape(-1, features), "tp", axis=0, tiled=True)
    gate_value = jnp.dot(pooled, gate_weight[0], preferred_element_type=jnp.float32)
    up_value = jnp.dot(pooled, up_weight[0], preferred_element_type=jnp.float32)
    hidden = (jax.nn.silu(gate_value) * up_value).astype(jnp.bfloat16)
    answers = lax.psum_scatter(
        jnp.dot(hidden, down_weight[0], preferred_element_type=jnp.float32).astype(jnp.bfloat16),
        "tp",
        scatter_dimension=0,
        tiled=True,
    )
    returned = lax.all_to_all(
        answers.reshape(expert_count, capacity, features),
        "sp",
        split_axis=0,
        concat_axis=0,
        tiled=True,
    )
    picked = jnp.take(returned.reshape(expert_count * capacity, features), placing, axis=0)
    picked = picked.reshape(own_rows, chosen_count, features).astype(jnp.float32)
    combined = jnp.sum(route_weight[:, :, None] * picked, axis=1)
    return (middle_wide + combined).astype(jnp.bfloat16)


def solution(mesh):
    placed = (
        P(("sp", "tp"), None),
        P("sp", "tp"),
        P("sp", "tp"),
        P("sp", "tp"),
        P("sp", "tp"),
        P("sp", "tp"),
        P("sp", "tp"),
        P("sp", "tp"),
        P("sp", "tp"),
        P(),
        P(),
        P(),
        P(("sp", "tp"), None),
        P(("sp", "tp"), None),
        P("sp", None, "tp"),
        P("sp", None, "tp"),
        P("sp", "tp", None),
    )
    return jax.shard_map(
        body, mesh=mesh, in_specs=placed, out_specs=P(("sp", "tp"), None), check_vma=False
    )
```

profile of v0, /device:TPU:0, one launch (start us, length us, event | category | flops | bytes accessed | tf_op | source)
XLA Modules:
  0.0 408.9 jit_solution(1248506105477989104)
XLA Ops:
  8.5 27.9 %all_gather.25 = f32[2048,2]{0,1:T(2,128)S(1)} all-gather(f32[256,2]{0,1:T(2,128)S(1)} %bitcast.168), channel_id=1, replica_groups=mesh['sp'=8,'tp'=4] {'sp'}, dimensions={0}, use_global_device_ids=true | all-gather | bytes 18432 | tf_op jit(solution)/shard_map/all_gather | solution.py:89
  38.3 19.0 %all_gather.22 = f32[2048,1]{0,1:T(1,128)S(1)} all-gather(f32[256,1]{0,1:T(1,128)S(1)} %reduce_window_sum.69), channel_id=1, replica_groups=mesh['sp'=8,'tp'=4] {'sp'}, dimensions={0}, use_global_device_ids=true | all-gather | bytes 9216 | tf_op jit(solution)/shard_map/all_gather | solution.py:88
  58.3 0.9 copy.47
  59.3 33.5 %all_gather.24 = bf16[2048,128]{0,1:T(8,128)(2,1)} all-gather(bf16[256,128]{0,1:T(8,128)(2,1)S(1)} %copy.47), channel_id=1, replica_groups=mesh['sp'=8,'tp'=4] {'sp'}, dimensions={0}, use_global_device_ids=true | all-gather | bytes 589824 | tf_op jit(solution)/shard_map/all_gather | solution.py:118
  92.8 0.9 copy.49
  93.7 31.4 %all_gather.26 = bf16[2048,128]{0,1:T(8,128)(2,1)S(1)} all-gather(bf16[256,128]{0,1:T(8,128)(2,1)S(1)} %copy.49), channel_id=1, replica_groups=mesh['sp'=8,'tp'=4] {'sp'}, dimensions={0}, use_global_device_ids=true | all-gather | bytes 589824 | tf_op jit(solution)/shard_map/all_gather | solution.py:119
  125.1 33.7 %all_gather.21 = bf16[2048,128]{1,0:T(8,128)(2,1)} all-gather(bf16[256,128]{1,0:T(8,128)(2,1)} %param.23), channel_id=1, replica_groups=mesh['sp'=8,'tp'=4] {'sp'}, dimensions={0}, use_global_device_ids=true | all-gather | bytes 589824 | tf_op jit(solution)/shard_map/all_gather | solution.py:116
  158.9 31.2 %all_gather.23 = bf16[2048,128]{1,0:T(8,128)(2,1)S(1)} all-gather(bf16[256,128]{1,0:T(8,128)(2,1)S(1)} %copy-done.5), channel_id=1, replica_groups=mesh['sp'=8,'tp'=4] {'sp'}, dimensions={0}, use_global_device_ids=true | all-gather | bytes 589824 | tf_op jit(solution)/shard_map/all_gather | solution.py:117
  192.3 10.5 %conditional.3 = (f32[1,128]{1,0:T(1,128)S(1)}, f32[1,128,128]{2,1,0:T(8,128)S(1)}, f32[2,128]{1,0:T(2,128)}, f32[2,128,64]{1,2,0:T(8,128)}) conditional(s32[]{:T(128)} %convert_element_type.106, (f32[1,128]{1,0:T(1,128)}, f32[1,128,128]{2,1,0:T(8,128)S(1)}, f32[2,128]{1,0:T(2,128)}, f32[2,128,64]{1,2,0:T(8,128)S(1)}) %tuple.35, (s32[]{:T(128)}, ...), branch_computations={%region_12.13_spmd, %region_13.18_spmd.clone} | conditional | flops 276104320 | bytes 15037726 | solution.py:170
  193.7 1.6 copy.51
  196.1 1.9 fusion.86
  198.4 1.3 multiply_add_fusion.1
  199.7 1.2 convolution_add_fusion.1
  203.3 8.7 %conditional.2 = ((f32[1,128]{1,0:T(1,128)}, f32[1,128,128]{2,1,0:T(8,128)S(1)}, f32[2,128]{1,0:T(2,128)}, f32[2,128,64]{1,2,0:T(8,128)S(1)})) conditional(s32[]{:T(128)} %convert_element_type.103, (f32[1,128]{1,0:T(1,128)}, f32[1,128,128]{2,1,0:T(8,128)S(1)}, f32[2,128]{1,0:T(2,128)}, f32[2,128,64]{1,2,0:T(8,128)S(1)}) %tuple.35, (s32[]{:T(128)}, ...), branch_computations={%region_6.7_spmd, %region_7.12_spmd.clone} | conditional | flops 276104320 | bytes 15033570 | solution.py:170
  204.3 0.9 copy.50
  205.2 1.9 fusion.84
  207.7 1.3 multiply_add_fusion
  210.8 1.2 bitcast_add_fusion
  214.7 2.5 fusion.38
  218.3 21.2 %reduce-scatter.3.cloned.1.call-done = bf16[64,2048]{1,0:T(8,128)(2,1)} async-done(((bf16[256,2048]{1,0:T(8,128)(2,1)}), bf16[64,2048]{1,0:T(8,128)(2,1)}) %reduce-scatter.3.cloned.1.call-update) | async-done | bytes 262160 | tf_op jit(solution)/shard_map/reduce_scatter | solution.py:192
  239.5 1.1 fusion.50
  240.7 1.4 convolution_convert_fusion.1
  242.2 31.1 %all_to_all.10 = bf16[8,32,2048]{2,1,0:T(8,128)(2,1)} all-to-all(bf16[8,32,2048]{2,1,0:T(8,128)(2,1)S(1)} %bitcast.150), channel_id=1, replica_groups=mesh['sp'=8,'tp'=4] {'sp'}, dimensions={0} | all-to-all | bytes 2097152 | tf_op jit(solution)/shard_map/all_to_all | solution.py:215
  273.6 32.5 %all-gather.2.cloned.1.call-done = bf16[1024,2048]{1,0:T(8,128)(2,1)} async-done(((bf16[256,2048]{1,0:T(8,128)(2,1)}), bf16[1024,2048]{1,0:T(8,128)(2,1)}) %all-gather.2.cloned.1.call-update) | async-done | bytes 4194320 | tf_op jit(solution)/shard_map/all_gather | solution.py:216
  306.0 4.5 %fusion.43 = f32[1024,256]{1,0:T(8,128)} fusion(bf16[1024,2048]{1,0:T(8,128)(2,1)} %all-gather.2.cloned.1.call-done, bf16[1,2048,256]{2,1,0:T(8,128)(2,1)S(1)} %copy-done.18), kind=kOutput, calls=%fused_computation.73 | convolution fusion | flops 1073741824 | bytes 6291456 | tf_op jit(solution)/shard_map/dot_general | solution.py:217
  310.5 9.4 %convolution_convert_fusion = bf16[1024,2048]{1,0:T(8,128)(2,1)} fusion(bf16[1024,2048]{1,0:T(8,128)(2,1)} %all-gather.2.cloned.1.call-done, bf16[1,256,2048]{2,1,0:T(8,128)(2,1)} %param.37, bf16[1,2048,256]{2,1,0:T(8,128)(2,1)} %param.36, f32[1024,256]{1,0:T(8,128)} %fusion.43), kind=kOutput, calls=%fused_computation.65 | convolution fusion | flops 2151153664 | bytes 11534336 | tf_op jit(solution)/shard_map/dot_general | solution.py:221
  320.0 44.7 %reduce-scatter.5.cloned.1.call-done = bf16[256,2048]{1,0:T(8,128)(2,1)} async-done(((bf16[1024,2048]{1,0:T(8,128)(2,1)}), bf16[256,2048]{1,0:T(8,128)(2,1)}) %reduce-scatter.5.cloned.1.call-update) | async-done | bytes 1048592 | tf_op jit(solution)/shard_map/reduce_scatter | solution.py:220
  364.7 5.5 %all-to-all-start.1 = ((bf16[8,32,2048]{2,1,0:T(8,128)(2,1)}), bf16[8,32,2048]{2,1,0:T(8,128)(2,1)S(1)}, u32[]{:S(2)}, u32[]{:S(2)}) async-start(bf16[8,32,2048]{2,1,0:T(8,128)(2,1)} %bitcast.151), calls=%async_computation.3 | async-start | bytes 2097152 | tf_op jit(solution)/shard_map/all_to_all | solution.py:226
  370.7 25.2 %all-to-all-done.1 = bf16[8,32,2048]{2,1,0:T(8,128)(2,1)S(1)} async-done(((bf16[8,32,2048]{2,1,0:T(8,128)(2,1)}), bf16[8,32,2048]{2,1,0:T(8,128)(2,1)S(1)}, u32[]{:S(2)}, u32[]{:S(2)}) %all-to-all-start.1) | async-done | bytes 1048608 | tf_op jit(solution)/shard_map/all_to_all | solution.py:226
  395.9 1.7 gather_fusion
  397.6 1.4 gather.7
  399.0 2.5 multiply_reduce_fusion
  (130 shorter events, 20.7 us)
Async XLA Ops:
  6.5 207.7 %copy-start = (bf16[512,2048]{1,0:T(8,128)(2,1)S(1)}, bf16[512,2048]{1,0:T(8,128)(2,1)}, u32[]{:S(2)}) copy-start(bf16[512,2048]{1,0:T(8,128)(2,1)} %param.30) | copy-start | bytes 6291460
  6.5 152.3 %copy-start.5 = (bf16[256,128]{1,0:T(8,128)(2,1)S(1)}, bf16[256,128]{1,0:T(8,128)(2,1)}, u32[]{:S(2)}) copy-start(bf16[256,128]{1,0:T(8,128)(2,1)} %param.24) | copy-start | bytes 196612
  6.5 233.0 %reduce-scatter.3.cloned.1.call-start = ((), (), s32[]{:S(2)}) async-start(), calls=%async_computation.4 | async-start | bytes 1310720 | tf_op jit(solution)/shard_map/reduce_scatter | solution.py:192
  192.9 0.6 copy-start.15
  195.3 2.6 copy-start.6
  198.0 2.9 copy-start.10
  198.0 3.0 copy-start.3
  198.0 3.0 copy-start.16
  198.0 3.0 copy-start.19
  199.7 1.8 copy-start.12
  202.8 0.5 copy-start.17
  203.4 3.8 copy-start.7
  207.2 2.3 copy-start.11
  207.2 2.4 copy-start.4
  207.2 2.4 copy-start.20
  208.9 1.2 copy-start.13
  214.7 2.7 copy-start.8
  214.7 24.9 %copy-start.1 = (bf16[64,2048]{1,0:T(8,128)(2,1)S(1)}, bf16[64,2048]{1,0:T(8,128)(2,1)}, u32[]{:S(2)}) copy-start(bf16[64,2048]{1,0:T(8,128)(2,1)} %param.21) | copy-start | bytes 786436
  214.7 26.0 %copy-start.9 = (f32[2048]{0:T(1024)S(1)}, f32[2048]{0:T(1024)}, u32[]{:S(2)}) copy-start(f32[2048]{0:T(1024)} %param.32) | copy-start | bytes 24580
  217.3 88.8 %all-gather.2.cloned.1.call-start = ((), (), s32[]{:S(2)}) async-start(), calls=%async_computation.5 | async-start | bytes 5242880 | tf_op jit(solution)/shard_map/all_gather | solution.py:216
  242.1 63.9 %copy-start.18 = (bf16[1,2048,256]{2,1,0:T(8,128)(2,1)S(1)}, bf16[1,2048,256]{2,1,0:T(8,128)(2,1)}, u32[]{:S(2)}) copy-start(bf16[1,2048,256]{2,1,0:T(8,128)(2,1)} %param.35) | copy-start | bytes 3145732
  273.3 91.4 %reduce-scatter.5.cloned.1.call-start = ((), (), s32[]{:S(2)}) async-start(), calls=%async_computation.6 | async-start | bytes 5242880 | tf_op jit(solution)/shard_map/reduce_scatter | solution.py:220
  320.0 50.6 %copy-start.14 = (f32[64,2]{0,1:T(2,128)S(1)}, f32[64,2]{0,1:T(2,128)}, u32[]{:S(2)}) copy-start(f32[64,2]{0,1:T(2,128)} %param.34) | copy-start | bytes 1540
  364.7 31.2 %all-to-all-start.1 = ((bf16[8,32,2048]{2,1,0:T(8,128)(2,1)}), bf16[8,32,2048]{2,1,0:T(8,128)(2,1)S(1)}, u32[]{:S(2)}, u32[]{:S(2)}) async-start(bf16[8,32,2048]{2,1,0:T(8,128)(2,1)} %bitcast.151), calls=%async_computation.3 | async-start | bytes 2097152 | tf_op jit(solution)/shard_map/all_to_all | solution.py:226
  397.6 4.0 copy-start.2
Sparse Core Ops, SparseCore 0:
  217.4 22.1 reduce-scatter.2
  273.5 32.5 all-gather.1
  320.1 44.5 reduce-scatter.4
where the time goes:
time: 410 us; the launch traced here: 409 us
  blocking collectives  208 us (51%)
  waiting for transfers between devices  124 us (30%)
  matrix products  25.6 us (6%)
  other arithmetic  18.2 us (4%)
  local copies, waits for them, and re-layouts  14.4 us (4%)
  between operations  13.4 us (3%)
  starting transfers between devices  5.77 us (1%)
    reduce_scatter x1, waiting for transfers between devices, body(): lax.psum_scatter(jnp.dot(hidden, down_weight[0], preferred_element_type=j...  44.7 us
    all_gather x1, blocking collectives, body(): keys_wide = lax.all_gather(key_wide, 'sp', axis=0, tiled=True)  33.7 us
    all_gather x1, blocking collectives, body(): keys_narrow = lax.all_gather(key_narrow, 'sp', axis=0, tiled=True)  33.5 us
    all_gather x1, waiting for transfers between devices, body(): lax.all_gather(arrived.reshape(-1, features), 'tp', axis=0, tiled=True)  32.5 us
    all_gather x1, blocking collectives, body(): values_narrow = lax.all_gather(value_narrow, 'sp', axis=0, tiled=True)  31.4 us
    all_gather x1, blocking collectives, body(): values_wide = lax.all_gather(value_wide, 'sp', axis=0, tiled=True)  31.2 us
    all_to_all x1, blocking collectives, body(): lax.all_to_all(outgoing, 'sp', split_axis=0, concat_axis=0, tiled=True)  31.1 us
    all_gather x1, blocking collectives, body(): lax.all_gather(running_narrow, 'sp', axis=0, tiled=True)  27.9 us
  transfers between devices with their start and end apart: 4, of which 4 were waited for; matrix products, arithmetic and copies ran while one was open for 0% of the time, Pallas kernels for 0%

commit v1 on v0

--- a/solution.py
+++ b/solution.py
@@ -113,7 +113,12 @@
         )
 
     state = (half_state(), half_state())
-    keys_wide = lax.all_gather(key_wide, "sp", axis=0, tiled=True)
+    ring = [key_wide]
+    for hop in range(7):
+        ring.append(lax.ppermute(ring[-1], "sp", [(dev, (dev + 1) % 8) for dev in range(8)]))
+    keys_wide = jnp.roll(
+        jnp.concatenate(ring[::-1], axis=0), (lax.axis_index("sp") + 1) * ring[0].shape[0], axis=0
+    )
     values_wide = lax.all_gather(value_wide, "sp", axis=0, tiled=True)
     keys_narrow = lax.all_gather(key_narrow, "sp", axis=0, tiled=True)
     values_narrow = lax.all_gather(value_narrow, "sp", axis=0, tiled=True)

time: 410 us -> 428 us (1.044)
  blocking collectives: 208 us -> 175 us
  waiting for transfers between devices: 124 us -> 153 us
  local copies, waits for them, and re-layouts: 14.4 us -> 28.1 us
    all_gather x1 -> x0, blocking collectives: 33.7 us -> none  [body(): keys_wide = lax.all_gather(key_wide, 'sp', axis=0, tiled=True)]
    ppermute x0 -> x7, waiting for transfers between devices: none -> 27.5 us  [body(): lax.ppermute(ring[-1], 'sp', [(dev, (dev + 1) % 8) for dev in range(8)])]
    unnamed x31 -> x58, local copies, waits for them, and re-layouts: 2.97 us -> 13.8 us
  transfers between devices with their start and end apart: 4 -> 11, of which waited for: 4 -> 9; matrix products, arithmetic and copies ran while one was open for 0% -> 4% of each run, Pallas kernels for 0% -> 0%
where the time goes in v1:
time: 428 us; the launch traced here: 427 us
  blocking collectives  175 us (41%)
  waiting for transfers between devices  153 us (36%)
  local copies, waits for them, and re-layouts  28.1 us (7%)
  matrix products  25.6 us (6%)
  other arithmetic  22.1 us (5%)
  between operations  13.4 us (3%)
  starting transfers between devices  8.87 us (2%)
    reduce_scatter x1, waiting for transfers between devices, body(): lax.psum_scatter(jnp.dot(hidden, down_weight[0], preferred_element_type=j...  44.7 us
    all_gather x1, blocking collectives, body(): keys_narrow = lax.all_gather(key_narrow, 'sp', axis=0, tiled=True)  33.6 us
    all_gather x1, waiting for transfers between devices, body(): lax.all_gather(arrived.reshape(-1, features), 'tp', axis=0, tiled=True)  32.5 us
    all_gather x1, blocking collectives, body(): values_narrow = lax.all_gather(value_narrow, 'sp', axis=0, tiled=True)  31.6 us
    all_gather x1, blocking collectives, body(): values_wide = lax.all_gather(value_wide, 'sp', axis=0, tiled=True)  31.4 us
    all_to_all x1, blocking collectives, body(): lax.all_to_all(outgoing, 'sp', split_axis=0, concat_axis=0, tiled=True)  31.1 us
    ppermute x7, waiting for transfers between devices, body(): lax.ppermute(ring[-1], 'sp', [(dev, (dev + 1) % 8) for dev in range(8)])  27.5 us
    all_gather x1, blocking collectives, body(): lax.all_gather(running_narrow, 'sp', axis=0, tiled=True)  26.4 us
  transfers between devices with their start and end apart: 11, of which 9 were waited for; matrix products, arithmetic and copies ran while one was open for 4% of the time, Pallas kernels for 0%

profile of v1, /device:TPU:0, one launch (start us, length us, event | category | flops | bytes accessed | tf_op | source)
XLA Modules:
  0.0 426.6 jit_solution(3495875526330565725)
XLA Ops:
  6.5 3.0 collective-permute-start
  11.3 26.4 %all_gather.21 = f32[2048,2]{0,1:T(2,128)S(1)} all-gather(f32[256,2]{0,1:T(2,128)S(1)} %bitcast.168), channel_id=1, replica_groups=mesh['sp'=8,'tp'=4] {'sp'}, dimensions={0}, use_global_device_ids=true | all-gather | bytes 18432 | tf_op jit(solution)/shard_map/all_gather | solution.py:89
  39.1 33.6 %all_gather.20 = bf16[2048,128]{0,1:T(8,128)(2,1)} all-gather(bf16[256,128]{0,1:T(8,128)(2,1)S(1)} %copy.47), channel_id=1, replica_groups=mesh['sp'=8,'tp'=4] {'sp'}, dimensions={0}, use_global_device_ids=true | all-gather | bytes 589824 | tf_op jit(solution)/shard_map/all_gather | solution.py:123
  73.6 31.6 %all_gather.22 = bf16[2048,128]{0,1:T(8,128)(2,1)S(1)} all-gather(bf16[256,128]{0,1:T(8,128)(2,1)S(1)} %copy.49), channel_id=1, replica_groups=mesh['sp'=8,'tp'=4] {'sp'}, dimensions={0}, use_global_device_ids=true | all-gather | bytes 589824 | tf_op jit(solution)/shard_map/all_gather | solution.py:124
  105.2 31.4 %all_gather.19 = bf16[2048,128]{1,0:T(8,128)(2,1)S(1)} all-gather(bf16[256,128]{1,0:T(8,128)(2,1)} %param.24), channel_id=1, replica_groups=mesh['sp'=8,'tp'=4] {'sp'}, dimensions={0}, use_global_device_ids=true | all-gather | bytes 589824 | tf_op jit(solution)/shard_map/all_gather | solution.py:122
  137.3 6.3 %collective-permute-done.1 = bf16[256,128]{1,0:T(8,128)(2,1)S(1)} collective-permute-done((bf16[256,128]{1,0:T(8,128)(2,1)S(1)}, bf16[256,128]{1,0:T(8,128)(2,1)S(1)}, u32[]{:S(2)}, u32[]{:S(2)}) %collective-permute-start.1) | collective-permute-done | bytes 65568 | tf_op jit(solution)/shard_map/ppermute | solution.py:118
  143.9 6.6 %collective-permute-done.2 = bf16[256,128]{1,0:T(8,128)(2,1)S(1)} collective-permute-done((bf16[256,128]{1,0:T(8,128)(2,1)S(1)}, bf16[256,128]{1,0:T(8,128)(2,1)S(1)}, u32[]{:S(2)}, u32[]{:S(2)}) %collective-permute-start.2) | collective-permute-done | bytes 65568 | tf_op jit(solution)/shard_map/ppermute | solution.py:118
  151.4 6.1 %collective-permute-done.3 = bf16[256,128]{1,0:T(8,128)(2,1)S(1)} collective-permute-done((bf16[256,128]{1,0:T(8,128)(2,1)S(1)}, bf16[256,128]{1,0:T(8,128)(2,1)S(1)}, u32[]{:S(2)}, u32[]{:S(2)}) %collective-permute-start.3) | collective-permute-done | bytes 65568 | tf_op jit(solution)/shard_map/ppermute | solution.py:118
  158.9 21.0 %all_gather.18 = f32[2048,1]{0,1:T(1,128)S(1)} all-gather(f32[256,1]{0,1:T(1,128)S(1)} %reduce_window_sum.69), channel_id=1, replica_groups=mesh['sp'=8,'tp'=4] {'sp'}, dimensions={0}, use_global_device_ids=true | all-gather | bytes 9216 | tf_op jit(solution)/shard_map/all_gather | solution.py:88
  181.2 1.3 copy.57
  182.4 1.3 reduce_window_sum.70
  184.5 6.4 %collective-permute-done.5 = bf16[256,128]{1,0:T(8,128)(2,1)} collective-permute-done((bf16[256,128]{1,0:T(8,128)(2,1)S(1)}, bf16[256,128]{1,0:T(8,128)(2,1)}, u32[]{:S(2)}, u32[]{:S(2)}) %collective-permute-start.5) | collective-permute-done | bytes 65568 | tf_op jit(solution)/shard_map/ppermute | solution.py:118
  193.6 1.3 add.311
  196.0 2.1 collective-permute-done.6
  207.1 9.9 %conditional.2 = (f32[1,128]{1,0:T(1,128)S(1)}, f32[1,128,128]{2,1,0:T(8,128)S(1)}, f32[2,128]{1,0:T(2,128)S(1)}, f32[2,128,64]{1,2,0:T(8,128)}) conditional(s32[]{:T(128)} %convert_element_type.103, (f32[1,128]{1,0:T(1,128)}, f32[1,128,128]{2,1,0:T(8,128)S(1)}, f32[2,128]{1,0:T(2,128)}, f32[2,128,64]{1,2,0:T(8,128)S(1)}) %tuple.35, ...), branch_computations={%region_6.7_spmd, %region_7.12_spmd.clone} | conditional | flops 276104320 | bytes 15037714 | solution.py:175
  208.5 1.6 copy.50
  210.9 1.9 fusion.84
  217.9 8.7 %conditional.3 = ((f32[1,128]{1,0:T(1,128)}, f32[1,128,128]{2,1,0:T(8,128)S(1)}, f32[2,128]{1,0:T(2,128)}, f32[2,128,64]{1,2,0:T(8,128)S(1)})) conditional(s32[]{:T(128)} %convert_element_type.106, (f32[1,128]{1,0:T(1,128)}, f32[1,128,128]{2,1,0:T(8,128)S(1)}, f32[2,128]{1,0:T(2,128)}, f32[2,128,64]{1,2,0:T(8,128)S(1)}) %tuple.35, ...), branch_computations={%region_12.13_spmd, %region_13.18_spmd.clone} | conditional | flops 276104320 | bytes 15033582 | solution.py:175
  219.8 1.9 fusion.86
  228.5 2.5 fusion.38
  232.1 23.2 %reduce-scatter.3.cloned.1.call-done = bf16[64,2048]{1,0:T(8,128)(2,1)} async-done(((bf16[256,2048]{1,0:T(8,128)(2,1)}), bf16[64,2048]{1,0:T(8,128)(2,1)}) %reduce-scatter.3.cloned.1.call-update) | async-done | bytes 262160 | tf_op jit(solution)/shard_map/reduce_scatter | solution.py:197
  256.5 1.4 convolution_convert_fusion.1
  257.9 31.1 %all_to_all.10 = bf16[8,32,2048]{2,1,0:T(8,128)(2,1)} all-to-all(bf16[8,32,2048]{2,1,0:T(8,128)(2,1)S(1)} %bitcast.150), channel_id=1, replica_groups=mesh['sp'=8,'tp'=4] {'sp'}, dimensions={0} | all-to-all | bytes 2097152 | tf_op jit(solution)/shard_map/all_to_all | solution.py:220
  289.3 32.5 %all-gather.2.cloned.1.call-done = bf16[1024,2048]{1,0:T(8,128)(2,1)} async-done(((bf16[256,2048]{1,0:T(8,128)(2,1)}), bf16[1024,2048]{1,0:T(8,128)(2,1)}) %all-gather.2.cloned.1.call-update) | async-done | bytes 4194320 | tf_op jit(solution)/shard_map/all_gather | solution.py:221
  321.8 4.5 %fusion.43 = f32[1024,256]{1,0:T(8,128)} fusion(bf16[1024,2048]{1,0:T(8,128)(2,1)} %all-gather.2.cloned.1.call-done, bf16[1,2048,256]{2,1,0:T(8,128)(2,1)S(1)} %copy-done.24), kind=kOutput, calls=%fused_computation.73 | convolution fusion | flops 1073741824 | bytes 6291456 | tf_op jit(solution)/shard_map/dot_general | solution.py:222
  326.3 9.4 %convolution_convert_fusion = bf16[1024,2048]{1,0:T(8,128)(2,1)} fusion(bf16[1024,2048]{1,0:T(8,128)(2,1)} %all-gather.2.cloned.1.call-done, bf16[1,256,2048]{2,1,0:T(8,128)(2,1)} %param.37, bf16[1,2048,256]{2,1,0:T(8,128)(2,1)} %param.36, f32[1024,256]{1,0:T(8,128)} %fusion.43), kind=kOutput, calls=%fused_computation.65 | convolution fusion | flops 2151153664 | bytes 11534336 | tf_op jit(solution)/shard_map/dot_general | solution.py:226
  335.7 44.7 %reduce-scatter.5.cloned.1.call-done = bf16[256,2048]{1,0:T(8,128)(2,1)} async-done(((bf16[1024,2048]{1,0:T(8,128)(2,1)}), bf16[256,2048]{1,0:T(8,128)(2,1)}) %reduce-scatter.5.cloned.1.call-update) | async-done | bytes 1048592 | tf_op jit(solution)/shard_map/reduce_scatter | solution.py:225
  380.5 5.5 %all-to-all-start.1 = ((bf16[8,32,2048]{2,1,0:T(8,128)(2,1)}), bf16[8,32,2048]{2,1,0:T(8,128)(2,1)S(1)}, u32[]{:S(2)}, u32[]{:S(2)}) async-start(bf16[8,32,2048]{2,1,0:T(8,128)(2,1)} %bitcast.151), calls=%async_computation.3 | async-start | bytes 2097152 | tf_op jit(solution)/shard_map/all_to_all | solution.py:231
  386.4 25.2 %all-to-all-done.1 = bf16[8,32,2048]{2,1,0:T(8,128)(2,1)S(1)} async-done(((bf16[8,32,2048]{2,1,0:T(8,128)(2,1)}), bf16[8,32,2048]{2,1,0:T(8,128)(2,1)S(1)}, u32[]{:S(2)}, u32[]{:S(2)}) %all-to-all-start.1) | async-done | bytes 1048608 | tf_op jit(solution)/shard_map/all_to_all | solution.py:231
  411.6 1.7 gather_fusion
  413.4 2.2 gather.7
  415.6 3.6 multiply_reduce_fusion
  (172 shorter events, 41.4 us)
Async XLA Ops:
  6.5 221.5 %copy-start = (bf16[512,2048]{1,0:T(8,128)(2,1)S(1)}, bf16[512,2048]{1,0:T(8,128)(2,1)}, u32[]{:S(2)}) copy-start(bf16[512,2048]{1,0:T(8,128)(2,1)} %param.30) | copy-start | bytes 6291460
  6.5 195.1 %copy-start.5 = (bf16[256,128]{1,0:T(8,128)(2,1)S(1)}, bf16[256,128]{1,0:T(8,128)(2,1)}, u32[]{:S(2)}) copy-start(bf16[256,128]{1,0:T(8,128)(2,1)} %param.23) | copy-start | bytes 196612
  6.5 137.1 %copy-start.20 = (f32[256,1]{0,1:T(1,128)S(1)}, f32[256,1]{0,1:T(1,128)}, u32[]{:S(2)}) copy-start(f32[256,1]{0,1:T(1,128)} %param.28) | copy-start | bytes 3076
  6.5 248.8 %reduce-scatter.3.cloned.1.call-start = ((), (), s32[]{:S(2)}) async-start(), calls=%async_computation.4 | async-start | bytes 1310720 | tf_op jit(solution)/shard_map/reduce_scatter | solution.py:197
  6.5 130.0 %collective-permute-start = (bf16[256,128]{1,0:T(8,128)(2,1)}, bf16[256,128]{1,0:T(8,128)(2,1)S(1)}, u32[]{:S(2)}, u32[]{:S(2)}) collective-permute-start(bf16[256,128]{1,0:T(8,128)(2,1)} %param.23), channel_id=1, source_target_pairs={{0,4},{4,8},{8,12},{12,16},{16,20},{20,24},{24,28},{28,0},{1,5},{5... | collective-permute-start | bytes 196616 | tf_op jit(solution)/shard_map/ppermute | solution.py:118
  136.6 7.0 %collective-permute-start.1 = (bf16[256,128]{1,0:T(8,128)(2,1)S(1)}, bf16[256,128]{1,0:T(8,128)(2,1)S(1)}, u32[]{:S(2)}, u32[]{:S(2)}) collective-permute-start(bf16[256,128]{1,0:T(8,128)(2,1)S(1)} %collective-permute-done), channel_id=1, source_target_pairs={{0,4},{4,8},{8,12},{12,16},{16,20},{20,24},{24,28},{28,0},{1,5},{5... | collective-permute-start | bytes 196616 | tf_op jit(solution)/shard_map/ppermute | solution.py:118
  143.6 7.0 %collective-permute-start.2 = (bf16[256,128]{1,0:T(8,128)(2,1)S(1)}, bf16[256,128]{1,0:T(8,128)(2,1)S(1)}, u32[]{:S(2)}, u32[]{:S(2)}) collective-permute-start(bf16[256,128]{1,0:T(8,128)(2,1)S(1)} %collective-permute-done.1), channel_id=1, source_target_pairs={{0,4},{4,8},{8,12},{12,16},{16,20},{20,24},{24,28},{28,0},{1,5},{5... | collective-permute-start | bytes 196616 | tf_op jit(solution)/shard_map/ppermute | solution.py:118
  143.9 7.5 %copy-start.18 = (f32[1,2,128]{2,1,0:T(2,128)}, f32[1,2,128]{2,1,0:T(2,128)S(1)}, u32[]{:S(2)}) copy-start(f32[1,2,128]{2,1,0:T(2,128)S(1)} %reduce-window.14) | copy-start | bytes 3076
  150.6 7.0 %collective-permute-start.3 = (bf16[256,128]{1,0:T(8,128)(2,1)S(1)}, bf16[256,128]{1,0:T(8,128)(2,1)S(1)}, u32[]{:S(2)}, u32[]{:S(2)}) collective-permute-start(bf16[256,128]{1,0:T(8,128)(2,1)S(1)} %collective-permute-done.2), channel_id=1, source_target_pairs={{0,4},{4,8},{8,12},{12,16},{16,20},{20,24},{24,28},{28,0},{1,5},{5... | collective-permute-start | bytes 196616 | tf_op jit(solution)/shard_map/ppermute | solution.py:118
  157.5 37.3 %copy-start.6 = (bf16[256,128]{1,0:T(8,128)(2,1)}, bf16[256,128]{1,0:T(8,128)(2,1)S(1)}, u32[]{:S(2)}) copy-start(bf16[256,128]{1,0:T(8,128)(2,1)S(1)} %collective-permute-done.3) | copy-start | bytes 196612
  157.5 26.2 %collective-permute-start.4 = (bf16[256,128]{1,0:T(8,128)(2,1)S(1)}, bf16[256,128]{1,0:T(8,128)(2,1)S(1)}, u32[]{:S(2)}, u32[]{:S(2)}) collective-permute-start(bf16[256,128]{1,0:T(8,128)(2,1)S(1)} %collective-permute-done.3), channel_id=1, source_target_pairs={{0,4},{4,8},{8,12},{12,16},{16,20},{20,24},{24,28},{28,0},{1,5},{5... | collective-permute-start | bytes 196616 | tf_op jit(solution)/shard_map/ppermute | solution.py:118
  183.8 11.1 %copy-start.7 = (bf16[256,128]{1,0:T(8,128)(2,1)}, bf16[256,128]{1,0:T(8,128)(2,1)S(1)}, u32[]{:S(2)}) copy-start(bf16[256,128]{1,0:T(8,128)(2,1)S(1)} %collective-permute-done.4) | copy-start | bytes 196612
  183.8 7.1 %collective-permute-start.5 = (bf16[256,128]{1,0:T(8,128)(2,1)S(1)}, bf16[256,128]{1,0:T(8,128)(2,1)}, u32[]{:S(2)}, u32[]{:S(2)}) collective-permute-start(bf16[256,128]{1,0:T(8,128)(2,1)S(1)} %collective-permute-done.4), channel_id=1, source_target_pairs={{0,4},{4,8},{8,12},{12,16},{16,20},{20,24},{24,28},{28,0},{1,5},{5... | collective-permute-start | bytes 196616 | tf_op jit(solution)/shard_map/ppermute | solution.py:118
  190.9 7.3 %collective-permute-start.6 = (bf16[256,128]{1,0:T(8,128)(2,1)}, bf16[256,128]{1,0:T(8,128)(2,1)}, u32[]{:S(2)}, u32[]{:S(2)}) collective-permute-start(bf16[256,128]{1,0:T(8,128)(2,1)} %collective-permute-done.5), channel_id=1, source_target_pairs={{0,4},{4,8},{8,12},{12,16},{16,20},{20,24},{24,28},{28,0},{1,5},{5... | collective-permute-start | bytes 196616 | tf_op jit(solution)/shard_map/ppermute | solution.py:118
  192.8 14.3 %copy-start.9 = (f32[2048,2]{0,1:T(2,128)S(1)}, f32[2048,2]{0,1:T(2,128)}, u32[]{:S(2)}) copy-start(f32[2048,2]{0,1:T(2,128)} %add.317) | copy-start | bytes 49156
  210.1 2.6 copy-start.10
  212.7 2.4 copy-start.14
  212.8 2.4 copy-start.3
  212.8 2.4 copy-start.22
  212.8 2.4 copy-start.25
  218.0 3.8 copy-start.11
  221.8 2.4 copy-start.4
  221.8 2.4 copy-start.26
  228.4 2.7 copy-start.12
  228.5 26.9 %copy-start.1 = (bf16[64,2048]{1,0:T(8,128)(2,1)S(1)}, bf16[64,2048]{1,0:T(8,128)(2,1)}, u32[]{:S(2)}) copy-start(bf16[64,2048]{1,0:T(8,128)(2,1)} %param.21) | copy-start | bytes 786436
  228.5 28.0 %copy-start.13 = (f32[2048]{0:T(1024)S(1)}, f32[2048]{0:T(1024)}, u32[]{:S(2)}) copy-start(f32[2048]{0:T(1024)} %param.32) | copy-start | bytes 24580
  231.1 90.7 %all-gather.2.cloned.1.call-start = ((), (), s32[]{:S(2)}) async-start(), calls=%async_computation.5 | async-start | bytes 5242880 | tf_op jit(solution)/shard_map/all_gather | solution.py:221
  257.9 63.9 %copy-start.24 = (bf16[1,2048,256]{2,1,0:T(8,128)(2,1)S(1)}, bf16[1,2048,256]{2,1,0:T(8,128)(2,1)}, u32[]{:S(2)}) copy-start(bf16[1,2048,256]{2,1,0:T(8,128)(2,1)} %param.35) | copy-start | bytes 3145732
  289.1 91.4 %reduce-scatter.5.cloned.1.call-start = ((), (), s32[]{:S(2)}) async-start(), calls=%async_computation.6 | async-start | bytes 5242880 | tf_op jit(solution)/shard_map/reduce_scatter | solution.py:225
  335.7 50.6 %copy-start.19 = (f32[64,2]{0,1:T(2,128)S(1)}, f32[64,2]{0,1:T(2,128)}, u32[]{:S(2)}) copy-start(f32[64,2]{0,1:T(2,128)} %param.34) | copy-start | bytes 1540
  380.5 31.2 %all-to-all-start.1 = ((bf16[8,32,2048]{2,1,0:T(8,128)(2,1)}), bf16[8,32,2048]{2,1,0:T(8,128)(2,1)S(1)}, u32[]{:S(2)}, u32[]{:S(2)}) async-start(bf16[8,32,2048]{2,1,0:T(8,128)(2,1)} %bitcast.151), calls=%async_computation.3 | async-start | bytes 2097152 | tf_op jit(solution)/shard_map/all_to_all | solution.py:231
  413.3 5.9 %copy-start.2 = (bf16[64,2048]{1,0:T(8,128)(2,1)S(1)}, bf16[64,2048]{1,0:T(8,128)(2,1)}, u32[]{:S(2)}) copy-start(bf16[64,2048]{1,0:T(8,128)(2,1)} %reduce-scatter.3.cloned.1.call-done) | copy-start | bytes 786436
  (6 other events, 7.3 us)
Sparse Core Ops, SparseCore 0:
  231.2 24.1 reduce-scatter.2
  289.2 32.5 all-gather.1
  335.8 44.5 reduce-scatter.4
